TPU v7x, 256 devices: a whole 4x4x8 slice. The times are simulated.
256 devices in a mesh: fs: 32 (over z, x), tp: 8 (over y, core).
Axes of the slice: x: 4, y: 4, z: 8, core: 2. Of those that a mesh axis runs over, the one named last changes fastest.
Arguments:
- normed_input: bfloat16 [65536, 2048], P('fs'), may hold values from -6 to 6
- gate_cotangent: bfloat16 [65536, 2048], P('fs', 'tp'), may hold values from -0.0625 to 0.0625
- first_value_cot: bfloat16 [65536, 1024], P('fs', 'tp'), may hold values from -0.0625 to 0.0625
- second_value_cot: bfloat16 [65536, 1024], P('fs', 'tp'), may hold values from -0.0625 to 0.0625
- head_lambda: float32 [8], P('tp'), may hold values from 0.3 to 0.8
- projection: bfloat16 [2048, 256], replicated, may hold values from -1 to 1, as said below
- gate_weight: float32 [2048, 2048], P('fs', 'tp'), may hold values from -0.125 to 0.125
- gate_first: float32 [256, 2048], P('fs', 'tp'), may hold values from -1.5 to 1.5
- gate_second: float32 [256, 2048], P('fs', 'tp'), may hold values from 0.01 to 1
- value_weight: float32 [2048, 1024], P('fs', 'tp'), may hold values from -0.125 to 0.125
- value_first: float32 [256, 1024], P('fs', 'tp'), may hold values from -1.5 to 1.5
- value_second: float32 [256, 1024], P('fs', 'tp'), may hold values from 0.01 to 1
Outputs:
- new_gate_weight: float32 [2048, 2048], P('fs', 'tp')
- gate_step: float32 [2048, 2048], P('fs', 'tp')
- gate_copy: bfloat16 [2048, 2048], P(None, 'tp')
- new_gate_first: float32 [256, 2048], P('fs', 'tp')
- new_gate_second: float32 [256, 2048], P('fs', 'tp')
- new_value_weight: float32 [2048, 1024], P('fs', 'tp')
- value_step: float32 [2048, 1024], P('fs', 'tp')
- value_copy: bfloat16 [2048, 1024], P(None, 'tp')
- new_value_first: float32 [256, 1024], P('fs', 'tp')
- new_value_second: float32 [256, 1024], P('fs', 'tp')
Inputs may be any that keep to these rules, and one draw needn't show every extreme that they name: `projection`: a low-rank factor whose rows differ in scale.
All inputs are finite; a program needn't handle non-finite values.
Results may differ from a plain program's by a relative error of at most 0.0054.
Values may be sent and summed in bfloat16 or wider, within the bound.
A program may use at most 64 MiB of HBM per device.

v0:
```python
import functools

import jax
import jax.numpy as jnp
from jax import lax
from jax.sharding import Mesh
from jax.sharding import PartitionSpec as P

D = 2048
HEADS = 8
VDIM = 128
FS = ("fs_0", "fs_1")
FS_TP = ("fs_0", "fs_1", "tp_0", "tp_1")
TP = ("tp_0", "tp_1")


moment_decay = 0.9
square_decay = 0.95
adam_floor = 1e-08
learn_rate = 0.02
rms_floor = 0.1


def in_blocks(value, dim, devices):
    shape = value.shape
    blocks = value.reshape(*shape[:dim], devices, shape[dim] // devices, *shape[dim + 1 :])
    return jnp.moveaxis(blocks, dim, 0)


def sum_at_owner(value, axis, dim):
    devices = lax.axis_size(axis)
    blocks = lax.all_to_all(in_blocks(value, dim, devices), axis, 0, 0, tiled=True)
    return jnp.sum(blocks.astype(jnp.float32), axis=0)


def in_one_piece(arrays, axis, dim, along):
    ends, at = ([], 0)
    for a in arrays[:-1]:
        at += a.shape[along]
        ends.append(at)
    both = jnp.concatenate(arrays, axis=along)
    return tuple(jnp.split(sum_at_owner(both, axis, dim), ends, axis=along))


def in_one_piece_2(arrays, axis, dim, along):
    ends, at = ([], 0)
    for a in arrays[:-1]:
        at += a.shape[along]
        ends.append(at)
    both = jnp.concatenate(arrays, axis=along)
    return tuple(jnp.split(lax.all_gather(both, axis, axis=dim, tiled=True), ends, axis=along))


def one_axis_at_a_time(value, axes):
    return functools.reduce(lax.psum, axes, value)


def across_tokens(left, right, precision=None):
    return lax.dot_general(
        left,
        right,
        (((0,), (0,)), ((), ())),
        preferred_element_type=jnp.float32,
        precision=precision,
    )


def moments(first, second, low):
    new_first = moment_decay * first + (1.0 - moment_decay) * low
    new_second = square_decay * second + (1.0 - square_decay) * low * low
    return (new_first, new_second, new_first / (jnp.sqrt(new_second) + adam_floor))


def split_product(stacked, cotangent, factors):
    both = across_tokens(stacked, cotangent)
    return both[:factors] + both[factors:]


def per_device(
    normed_input,
    gate_cotangent,
    first_value_cot,
    second_value_cot,
    head_lambda,
    projection,
    gate_weight,
    gate_first,
    gate_second,
    value_weight,
    value_first,
    value_second,
):
    highest = lax.Precision.HIGHEST
    column_lambda = jnp.repeat(head_lambda, VDIM)
    value_cot = (
        first_value_cot.astype(jnp.float32)
        - column_lambda[None, :] * second_value_cot.astype(jnp.float32)
    ).astype(jnp.bfloat16)
    rows_here = gate_weight.shape[0]
    first_row = lax.axis_index(FS) * rows_here
    local_factor = lax.dynamic_slice_in_dim(projection, first_row, rows_here, 0).astype(jnp.float32)
    projected = jnp.dot(normed_input, projection, preferred_element_type=jnp.float32)
    upper = projected.astype(jnp.bfloat16)
    upper_wide = lax.optimization_barrier(upper).astype(jnp.float32)
    lower = (projected - upper_wide).astype(jnp.bfloat16)
    stacked = jnp.concatenate([upper, lower], axis=1)
    factors = projection.shape[1]
    partial_gate = split_product(stacked, gate_cotangent, factors)
    partial_value = split_product(stacked, value_cot, factors)
    gate_low, value_low = in_one_piece(
        (partial_gate.astype(jnp.bfloat16), partial_value.astype(jnp.bfloat16)), FS, 0, 1
    )
    new_gate_first, new_gate_second, gate_dir = moments(gate_first, gate_second, gate_low)
    new_value_first, new_value_second, value_dir = moments(value_first, value_second, value_low)
    pieces = in_one_piece_2((gate_dir, value_dir), FS, 0, 1)
    gate_update = jnp.dot(local_factor, pieces[0], precision=highest)
    value_update = jnp.dot(local_factor, pieces[1], precision=highest)
    gate_total, value_total = (
        one_axis_at_a_time(jnp.sum(gate_update * gate_update), FS_TP),
        one_axis_at_a_time(jnp.sum(value_update * value_update), FS_TP),
    )
    gate_step = gate_update / (jnp.sqrt(gate_total / (D * D)) + rms_floor)
    value_step = value_update / (jnp.sqrt(value_total / (D * HEADS * VDIM)) + rms_floor)
    new_gate_weight = gate_weight - learn_rate * gate_step
    new_value_weight = value_weight - learn_rate * value_step
    gate_copy, value_copy = in_one_piece_2(
        (new_gate_weight.astype(jnp.bfloat16), new_value_weight.astype(jnp.bfloat16)), FS, 0, 1
    )
    return (
        new_gate_weight,
        gate_step,
        gate_copy,
        new_gate_first,
        new_gate_second,
        new_value_weight,
        value_step,
        value_copy,
        new_value_first,
        new_value_second,
    )


def solution(mesh):
    torus = Mesh(mesh.devices.reshape(8, 4, 4, 2), ("fs_0", "fs_1", "tp_0", "tp_1"))
    placed = (
        P(FS, None),
        P(FS, TP),
        P(FS, TP),
        P(FS, TP),
        P(TP),
        P(),
        P(FS, TP),
        P(FS, TP),
        P(FS, TP),
        P(FS, TP),
        P(FS, TP),
        P(FS, TP),
    )
    return jax.shard_map(
        per_device,
        mesh=torus,
        in_specs=placed,
        out_specs=(
            P(FS, TP),
            P(FS, TP),
            P(None, TP),
            P(FS, TP),
            P(FS, TP),
            P(FS, TP),
            P(FS, TP),
            P(None, TP),
            P(FS, TP),
            P(FS, TP),
        ),
        check_vma=False,
    )
```

profile of v0, /device:TPU:1, one launch (start us, length us, event | category | flops | bytes accessed | tf_op | source)
XLA Modules:
  0.0 214.5 jit_solution(6516814320399428015)
XLA Ops:
  7.2 0.0 copy-start
  7.2 1.2 copy-done
  8.4 5.8 %fusion.21 = (bf16[2048,256]{0,1:T(8,128)(2,1)S(1)}, f32[2048,256]{0,1:T(8,128)S(1)}) fusion(bf16[2048,2048]{1,0:T(8,128)(2,1)} %param.12, bf16[2048,256]{1,0:T(8,128)(2,1)S(1)} %copy-done), kind=kOutput, calls=%fused_computation.40 | convolution fusion | flops 2148007936 | bytes 12582912 | tf_op jit(solution)/shard_map/dot_general | solution.py:102
  14.2 0.0 copy-start.7
  14.2 0.3 subtract_convert_fusion
  14.5 0.9 copy-done.7
  15.4 0.0 copy-start.8
  15.4 0.0 copy-start.9
  15.4 0.8 fusion.1
  16.8 0.0 copy-done.8
  16.9 0.0 copy-done.9
  16.9 0.0 copy-start.3
  16.9 0.0 copy-start.4
  16.9 0.0 copy-start.5
  16.9 0.0 copy-start.6
  16.9 0.8 fusion
  17.8 0.0 copy-start.2
  17.8 0.0 copy-start.1
  17.8 0.8 copy.22
  18.7 11.9 %all-to-all-start = ((bf16[32,8,384]{2,1,0:T(8,128)(2,1)}), bf16[32,8,384]{2,1,0:T(8,128)(2,1)S(1)}, u32[]{:S(2)}, u32[]{:S(2)}) async-start(bf16[32,8,384]{2,1,0:T(8,128)(2,1)} %bitcast.1), calls=%async_computation | async-start | bytes 393216 | tf_op jit(solution)/shard_map/all_to_all | solution.py:32
  30.5 0.0 all-gather.2.cloned.1.call-start
  30.6 9.9 %all-to-all-done = bf16[32,8,384]{2,1,0:T(8,128)(2,1)S(1)} async-done(((bf16[32,8,384]{2,1,0:T(8,128)(2,1)}), bf16[32,8,384]{2,1,0:T(8,128)(2,1)S(1)}, u32[]{:S(2)}, u32[]{:S(2)}) %all-to-all-start) | async-done | bytes 196640 | tf_op jit(solution)/shard_map/all_to_all | solution.py:32
  40.5 0.0 copy-done.3
  40.5 0.0 copy-done.4
  40.6 0.6 add_divide_fusion
  41.2 0.0 copy-done.5
  41.2 0.0 copy-done.6
  41.2 0.6 add_divide_fusion.1
  41.8 35.5 %all_gather.6 = f32[256,384]{1,0:T(8,128)S(1)} all-gather(f32[8,384]{1,0:T(8,128)S(1)} %pad_maximum_fusion.5), channel_id=1, replica_groups=mesh['fs_0'=8,'fs_1'=4,'tp_0'=4,'tp_1'=2] {'fs_0','fs_1'}, dimensions={0}, use_global_device_ids=true | all-gather | bytes 405504 | tf_op jit(solution)/shard_map/all_gather | solution.py:51
  77.2 0.8 multiply_reduce_fusion
  78.1 0.8 multiply_reduce_fusion.1
  78.9 13.2 %all-reduce = (f32[]{:T(128)}, f32[]{:T(128)}) all-reduce(f32[]{:T(128)} %get-tuple-element.32, f32[]{:T(128)} %get-tuple-element.34), channel_id=1, replica_groups=mesh['fs_0'=8,'fs_1'=4,'tp_0'=4,'tp_1'=2] {'fs_0'}, use_global_device_ids=true, to_apply=%region_2.0 | all-reduce | flops 2 | bytes 16 | tf_op jit(solution)/shard_map/psum | solution.py:55
  92.1 7.5 %all-reduce.2 = (f32[]{:T(128)}, f32[]{:T(128)}) all-reduce(f32[]{:T(128)} %get-tuple-element.10, f32[]{:T(128)} %get-tuple-element.11), channel_id=1, replica_groups=mesh['fs_0'=8,'fs_1'=4,'tp_0'=4,'tp_1'=2] {'fs_1'}, use_global_device_ids=true, to_apply=%region_3.0 | all-reduce | flops 2 | bytes 16 | tf_op jit(solution)/shard_map/psum | solution.py:55
  99.5 9.3 %all-reduce.1 = (f32[]{:T(128)}, f32[]{:T(128)}) all-reduce(f32[]{:T(128)} %get-tuple-element.14, f32[]{:T(128)} %get-tuple-element.15), channel_id=1, replica_groups=mesh['fs_0'=8,'fs_1'=4,'tp_0'=4,'tp_1'=2] {'tp_0'}, use_global_device_ids=true, to_apply=%region_4.0 | all-reduce | flops 2 | bytes 16 | tf_op jit(solution)/shard_map/psum | solution.py:55
  108.9 25.2 %all-reduce.3 = (f32[]{:T(128)}, f32[]{:T(128)}) all-reduce(f32[]{:T(128)} %get-tuple-element.12, f32[]{:T(128)} %get-tuple-element.13), channel_id=1, replica_groups=mesh['fs_0'=8,'fs_1'=4,'tp_0'=4,'tp_1'=2] {'tp_1'}, use_global_device_ids=true, to_apply=%region_5.0 | all-reduce | flops 2 | bytes 16 | tf_op jit(solution)/shard_map/psum | solution.py:55
  135.5 0.0 copy-done.2
  135.5 0.6 fusion.18
  136.1 0.0 copy-done.1
  136.1 0.7 fusion.17
  136.8 0.6 pad_maximum_fusion.4
  137.4 0.0 all-gather.2.cloned.1.call-update
  137.4 66.0 %all-gather.2.cloned.1.call-done = bf16[2048,384]{1,0:T(8,128)(2,1)} async-done(((bf16[64,384]{1,0:T(8,128)(2,1)}), bf16[2048,384]{1,0:T(8,128)(2,1)}) %all-gather.2.cloned.1.call-update) | async-done | bytes 1572880 | tf_op jit(solution)/shard_map/all_gather | solution.py:51
  203.5 2.3 %split.28 = bf16[2048,256]{1,0:T(8,128)(2,1)} slice(bf16[2048,384]{1,0:T(8,128)(2,1)} %all-gather.2.cloned.1.call-done), slice={[0:2048], [0:256]} | slice | bytes 2097152 | tf_op jit(solution)/shard_map/split | solution.py:51
  205.7 1.9 split.29
  (5 shorter events, 0.1 us)
Async XLA Ops:
  7.2 1.2 copy-start
  14.2 1.2 copy-start.7
  15.4 1.5 copy-start.8
  15.4 1.5 copy-start.9
  16.9 23.7 %copy-start.3 = (f32[8,256]{1,0:T(8,128)S(1)}, f32[8,256]{1,0:T(8,128)}, u32[]{:S(2)}) copy-start(f32[8,256]{1,0:T(8,128)} %param.20) | copy-start | bytes 24580
  16.9 23.7 %copy-start.4 = (f32[8,256]{1,0:T(8,128)S(1)}, f32[8,256]{1,0:T(8,128)}, u32[]{:S(2)}) copy-start(f32[8,256]{1,0:T(8,128)} %param.19) | copy-start | bytes 24580
  16.9 24.3 %copy-start.5 = (f32[8,128]{1,0:T(8,128)S(1)}, f32[8,128]{1,0:T(8,128)}, u32[]{:S(2)}) copy-start(f32[8,128]{1,0:T(8,128)} %param.23) | copy-start | bytes 12292
  16.9 24.3 %copy-start.6 = (f32[8,128]{1,0:T(8,128)S(1)}, f32[8,128]{1,0:T(8,128)}, u32[]{:S(2)}) copy-start(f32[8,128]{1,0:T(8,128)} %param.22) | copy-start | bytes 12292
  17.8 117.7 %copy-start.2 = (f32[64,128]{1,0:T(8,128)S(1)}, f32[64,128]{1,0:T(8,128)}, u32[]{:S(2)}) copy-start(f32[64,128]{1,0:T(8,128)} %param.21) | copy-start | bytes 98308
  17.8 118.4 %copy-start.1 = (f32[64,256]{1,0:T(8,128)S(1)}, f32[64,256]{1,0:T(8,128)}, u32[]{:S(2)}) copy-start(f32[64,256]{1,0:T(8,128)} %param.18) | copy-start | bytes 196612
  18.7 21.8 %all-to-all-start = ((bf16[32,8,384]{2,1,0:T(8,128)(2,1)}), bf16[32,8,384]{2,1,0:T(8,128)(2,1)S(1)}, u32[]{:S(2)}, u32[]{:S(2)}) async-start(bf16[32,8,384]{2,1,0:T(8,128)(2,1)} %bitcast.1), calls=%async_computation | async-start | bytes 393216 | tf_op jit(solution)/shard_map/all_to_all | solution.py:32
  30.5 173.0 %all-gather.2.cloned.1.call-start = ((), (), s32[]{:S(2)}) async-start(), calls=%async_computation.1 | async-start | bytes 1622016 | tf_op jit(solution)/shard_map/all_gather | solution.py:51
Sparse Core Ops, SparseCore 0:
  137.6 65.8 all-gather.1
where the time goes:
time: 219 us; the launch traced here: 214 us
  blocking collectives  90.7 us (41%)
  waiting for transfers between devices  76 us (35%)
  between operations  16.3 us (7%)
  starting transfers between devices  11.9 us (5%)
  matrix products  8.97 us (4%)
  local copies, waits for them, and re-layouts  7.14 us (3%)
  other arithmetic  3.52 us (2%)
    all_gather x1, waiting for transfers between devices, in_one_piece_2(): lax.all_gather(both, axis, axis=dim, tiled=True)  66 us
    psum x4, blocking collectives, one_axis_at_a_time(): return functools.reduce(lax.psum, axes, value)  55.2 us
    all_gather x1, blocking collectives, in_one_piece_2(): lax.all_gather(both, axis, axis=dim, tiled=True)  35.5 us
    all_to_all x1, starting transfers between devices, sum_at_owner(): lax.all_to_all(in_blocks(value, dim, devices), axis, 0, 0, tiled=True)  11.9 us
    all_to_all x1, waiting for transfers between devices, sum_at_owner(): lax.all_to_all(in_blocks(value, dim, devices), axis, 0, 0, tiled=True)  9.92 us
    dot_general x1, matrix products, per_device(): jnp.dot(normed_input, projection, preferred_element_type=jnp.float32)  5.75 us
  transfers between devices with their start and end apart: 2, of which 2 were waited for; matrix products, arithmetic and copies ran while one was open for 0% of the time, Pallas kernels for 0%

commit v1 on v0

v1 whole, which is shorter than its diff:
```python
import functools

import jax
import jax.numpy as jnp
from jax import lax
from jax.experimental import pallas as pl
from jax.experimental.pallas import tpu as pltpu
from jax.sharding import Mesh
from jax.sharding import PartitionSpec as P

D = 2048
RANK = 256
GATE = 256
VALUE = 128
BOTH = GATE + VALUE
NZ, NX, NY, NC = 8, 4, 4, 2
FS = ("z", "x")
TP = ("y", "c")
AXES = ("z", "x", "y", "c")
OWN = RANK // (NZ * NX)
ROWS = D // (NZ * NX)
TOKENS = 2048
CHUNKS = 4
CHUNK = TOKENS // CHUNKS

moment_decay = 0.9
square_decay = 0.95
adam_floor = 1e-08
learn_rate = 0.02
rms_floor = 0.1

MESH = pl.DeviceIdType.MESH
f32 = jnp.float32
bf16 = jnp.bfloat16


def moments(first, second, low):
    new_first = moment_decay * first + (1.0 - moment_decay) * low
    new_second = square_decay * second + (1.0 - square_decay) * low * low
    return new_first, new_second


def exchange_kernel(
    x_hbm, gate_hbm, one_hbm, two_hbm, lam_ref, proj_hbm, gw_hbm, vw_hbm, gf_hbm, gs_hbm, vf_hbm, vs_hbm,
    low_ref, upd_ref, wall_ref, tot_ref,
    xbuf, gbuf, onebuf, twobuf, pbuf, gwbuf, vwbuf, gfbuf, gsbuf, vfbuf, vsbuf,
    acc, part, landed, dirs,
    in_sems, x_sems, w_send, w_recv, rs_sems, ag_sems, tot_sems,
):
    z, x, y, c = [lax.axis_index(a) for a in AXES]
    me = z * NX + x
    my_tp = y * NC + c

    def at(dz, dx):
        return (lax.rem(z + dz, NZ), lax.rem(x + dx, NX), y, c)

    offsets = [(dz, dx) for dz in range(NZ) for dx in range(NX) if (dz, dx) != (0, 0)]
    tp_offsets = [(dy, dc) for dy in range(NY) for dc in range(NC) if (dy, dc) != (0, 0)]

    def tp_at(dy, dc):
        return (z, x, lax.rem(y + dy, NY), lax.rem(c + dc, NC))

    loads = [
        pltpu.make_async_copy(src, dst, in_sems.at[i])
        for i, (src, dst) in enumerate([
            (gw_hbm, gwbuf), (vw_hbm, vwbuf), (proj_hbm, pbuf), (gate_hbm, gbuf), (one_hbm, onebuf),
            (two_hbm, twobuf), (gf_hbm, gfbuf), (gs_hbm, gsbuf), (vf_hbm, vfbuf), (vs_hbm, vsbuf),
        ])
    ]
    x_loads = [
        pltpu.make_async_copy(
            x_hbm.at[pl.ds(i * CHUNK, CHUNK)], xbuf.at[pl.ds(i * CHUNK, CHUNK)], x_sems.at[i])
        for i in range(CHUNKS)
    ]
    for copy in loads[:3]:
        copy.start()
    x_loads[0].start()
    for copy in loads[3:6]:
        copy.start()
    for copy in x_loads[1:]:
        copy.start()
    for copy in loads[6:]:
        copy.start()

    barrier = pltpu.get_barrier_semaphore()
    for dz, dx in offsets:
        pl.semaphore_signal(barrier, inc=1, device_id=at(dz, dx), device_id_type=MESH)
    for dy, dc in tp_offsets:
        pl.semaphore_signal(barrier, inc=1, device_id=tp_at(dy, dc), device_id_type=MESH)

    loads[0].wait()
    loads[1].wait()
    wall_ref[x, z, :, 0:GATE] = gwbuf[...].astype(bf16)
    wall_ref[x, z, :, GATE:BOTH] = vwbuf[...].astype(bf16)
    loads[2].wait()

    pl.semaphore_wait(barrier, len(offsets) + len(tp_offsets))

    def remote(src, dst, send, recv, device):
        return pltpu.make_async_remote_copy(
            src_ref=src, dst_ref=dst, send_sem=send, recv_sem=recv, device_id=device, device_id_type=MESH)

    up, down = at(1, 0), at(NZ - 1, 0)
    east, west = at(0, 1), at(0, NX - 1)
    w_copies = []

    def w_step(step):
        pair = []
        for way, device in ((0, up), (1, down)):
            slot = lax.rem(z + (NZ - step if way == 0 else step), NZ)
            block = wall_ref.at[x, slot]
            if step == NZ // 2 - 1:
                block = block.at[pl.ds(way * (ROWS // 2), ROWS // 2)]
            pair.append(remote(block, block, w_send.at[2 * step + way], w_recv.at[2 * step + way], device))
        for copy in pair:
            copy.start()
        w_copies.append(pair)

    def w_landed(step):
        for copy in w_copies[step]:
            copy.wait_recv()

    w_step(0)

    def chunk(i):
        x_loads[i].wait()
        if i == 0:
            for copy in loads[3:6]:
                copy.wait()
        rows = pl.ds(i * CHUNK, CHUNK)
        projected = jnp.dot(xbuf[rows, :], pbuf[...], preferred_element_type=f32).astype(bf16)
        value_cot = (onebuf[rows, :].astype(f32) - lam_ref[0] * twobuf[rows, :].astype(f32)).astype(bf16)
        both = jnp.concatenate([gbuf[rows, :], value_cot], axis=1)
        term = lax.dot_general(projected, both, (((0,), (0,)), ((), ())), preferred_element_type=f32)
        if i == 0:
            acc[...] = term
        else:
            acc[...] += term

    chunk(0)
    w_landed(0)
    w_step(1)
    chunk(1)
    w_landed(1)
    w_step(2)
    chunk(2)
    w_landed(2)
    w_step(3)
    chunk(3)

    part[...] = acc[...].reshape(NZ * NX, OWN, BOTH).astype(bf16)
    rs_copies = []
    for j, (dz, dx) in enumerate(offsets):
        device = at(dz, dx)
        owner = device[0] * NX + device[1]
        rs_copies.append(remote(part.at[owner], landed.at[me], rs_sems.at[0, j], rs_sems.at[1, j], device))
        rs_copies[-1].start()
    for copy in loads[6:]:
        copy.wait()
    landed[me] = part[me]

    w_landed(3)
    column = wall_ref.at[x]
    x_copies = [
        remote(column, column, w_send.at[8], w_recv.at[8], east),
        remote(column, column, w_send.at[9], w_recv.at[9], west),
    ]

    for copy in rs_copies:
        copy.wait_recv()
    low = jnp.sum(landed[...].astype(f32), axis=0)
    low_ref[...] = low
    gate_first, gate_second = moments(gfbuf[...], gsbuf[...], low[:, 0:GATE])
    value_first, value_second = moments(vfbuf[...], vsbuf[...], low[:, GATE:BOTH])
    dirs[me, :, 0:GATE] = (gate_first / (jnp.sqrt(gate_second) + adam_floor)).astype(bf16)
    dirs[me, :, GATE:BOTH] = (value_first / (jnp.sqrt(value_second) + adam_floor)).astype(bf16)
    ag_copies = []
    for j, (dz, dx) in enumerate(offsets):
        ag_copies.append(remote(dirs.at[me], dirs.at[me], ag_sems.at[0, j], ag_sems.at[1, j], at(dz, dx)))
        ag_copies[-1].start()
    for copy in x_copies:
        copy.start()
    for copy in ag_copies:
        copy.wait_recv()

    spread = dirs[...].astype(f32).reshape(RANK, BOTH).astype(bf16)
    gate_sum = jnp.zeros((8, 128), f32)
    value_sum = jnp.zeros((8, 128), f32)
    for i in range(4):
        rows = pl.ds(i * 512, 512)
        update = jnp.dot(pbuf[rows, :], spread, preferred_element_type=f32)
        upd_ref[rows, :] = update
        squares = (update * update).reshape(64, 8, BOTH).sum(axis=0)
        gate_sum += squares[:, 0:128] + squares[:, 128:256]
        value_sum += squares[:, 256:384]
    tot_ref[my_tp, :, 0:128] = gate_sum
    tot_ref[my_tp, :, 128:256] = value_sum
    tot_copies = []
    for j, (dy, dc) in enumerate(tp_offsets):
        tot_copies.append(
            remote(tot_ref.at[my_tp], tot_ref.at[my_tp], tot_sems.at[0, j], tot_sems.at[1, j], tp_at(dy, dc)))
        tot_copies[-1].start()

    for copy in x_copies:
        copy.wait_recv()
    half = NZ // 2
    from_west = wall_ref.at[lax.rem(x + NX - 1, NX), pl.ds(0, half)]
    from_east = wall_ref.at[lax.rem(x + 1, NX), pl.ds(half, half)]
    far_copies = [
        remote(from_west, from_west, w_send.at[10], w_recv.at[10], east),
        remote(from_east, from_east, w_send.at[11], w_recv.at[11], west),
    ]
    for copy in far_copies:
        copy.start()
    for copy in tot_copies:
        copy.wait_recv()
    for copy in far_copies:
        copy.wait_recv()
    for pair in w_copies:
        for copy in pair:
            copy.wait_send()
    for copy in rs_copies + ag_copies + x_copies + far_copies + tot_copies:
        copy.wait_send()


def finish_kernel(
    low_ref, upd_ref, wall_ref, tot_ref, gw_ref, vw_ref, gf_ref, gs_ref, vf_ref, vs_ref,
    ngw_ref, gstep_ref, gcopy_hbm, ngf_ref, ngs_ref, nvw_ref, vstep_ref, vcopy_hbm, nvf_ref, nvs_ref,
    gout, vout, sems,
):
    z, x = lax.axis_index("z"), lax.axis_index("x")
    first_row = (z * NX + x) * ROWS
    totals = jnp.sum(tot_ref[...], axis=(0, 1))
    gate_total = jnp.sum(totals[0:128])
    value_total = jnp.sum(totals[128:256])
    gate_scale = 1.0 / (jnp.sqrt(jnp.full((8, 128), gate_total, f32) / (D * D)) + rms_floor)
    value_scale = 1.0 / (jnp.sqrt(jnp.full((8, 128), value_total, f32) / (D * 8 * VALUE)) + rms_floor)
    gate_scale = jnp.max(gate_scale)
    value_scale = jnp.max(value_scale)
    copies = []
    for f in range(NZ * NX):
        rows = pl.ds(f * ROWS, ROWS)
        update = upd_ref[rows, :]
        old = wall_ref[f % NX, f // NX].astype(f32)
        gout[rows, :] = (old[:, 0:GATE] - learn_rate * (update[:, 0:GATE] * gate_scale)).astype(bf16)
        vout[rows, :] = (old[:, GATE:BOTH] - learn_rate * (update[:, GATE:BOTH] * value_scale)).astype(bf16)
        if f % 8 == 7:
            span = pl.ds((f - 7) * ROWS, 8 * ROWS)
            n = f // 8
            copies.append(pltpu.make_async_copy(gout.at[span], gcopy_hbm.at[span], sems.at[2 * n]))
            copies.append(pltpu.make_async_copy(vout.at[span], vcopy_hbm.at[span], sems.at[2 * n + 1]))
            copies[-2].start()
            copies[-1].start()
    mine = upd_ref[pl.ds(pl.multiple_of(first_row, ROWS), ROWS), :]
    gate_step = mine[:, 0:GATE] * gate_scale
    value_step = mine[:, GATE:BOTH] * value_scale
    gstep_ref[...] = gate_step
    vstep_ref[...] = value_step
    ngw_ref[...] = gw_ref[...] - learn_rate * gate_step
    nvw_ref[...] = vw_ref[...] - learn_rate * value_step
    ngf_ref[...], ngs_ref[...] = moments(gf_ref[...], gs_ref[...], low_ref[:, 0:GATE])
    nvf_ref[...], nvs_ref[...] = moments(vf_ref[...], vs_ref[...], low_ref[:, GATE:BOTH])
    for copy in copies:
        copy.wait()


def per_device(
    normed_input, gate_cotangent, first_value_cot, second_value_cot, head_lambda, projection,
    gate_weight, gate_first, gate_second, value_weight, value_first, value_second,
):
    hbm = pl.BlockSpec(memory_space=pltpu.HBM)
    vmem = pl.BlockSpec(memory_space=pltpu.VMEM)
    smem = pl.BlockSpec(memory_space=pltpu.SMEM)
    peers = NZ * NX - 1
    low, upd, wall, tot = pl.pallas_call(
        exchange_kernel,
        name="exchange",
        in_specs=[hbm, hbm, hbm, hbm, smem, hbm, hbm, hbm, hbm, hbm, hbm, hbm],
        out_specs=[vmem] * 4,
        out_shape=[
            jax.ShapeDtypeStruct((OWN, BOTH), f32),
            jax.ShapeDtypeStruct((D, BOTH), f32),
            jax.ShapeDtypeStruct((NX, NZ, ROWS, BOTH), bf16),
            jax.ShapeDtypeStruct((NY * NC, 8, 256), f32),
        ],
        scratch_shapes=[
            pltpu.VMEM((TOKENS, D), bf16),
            pltpu.VMEM((TOKENS, GATE), bf16),
            pltpu.VMEM((TOKENS, VALUE), bf16),
            pltpu.VMEM((TOKENS, VALUE), bf16),
            pltpu.VMEM((D, RANK), bf16),
            pltpu.VMEM((ROWS, GATE), f32),
            pltpu.VMEM((ROWS, VALUE), f32),
            pltpu.VMEM((OWN, GATE), f32),
            pltpu.VMEM((OWN, GATE), f32),
            pltpu.VMEM((OWN, VALUE), f32),
            pltpu.VMEM((OWN, VALUE), f32),
            pltpu.VMEM((RANK, BOTH), f32),
            pltpu.VMEM((NZ * NX, OWN, BOTH), bf16),
            pltpu.VMEM((NZ * NX, OWN, BOTH), bf16),
            pltpu.VMEM((NZ * NX, OWN, BOTH), bf16),
            pltpu.SemaphoreType.DMA((10,)),
            pltpu.SemaphoreType.DMA((CHUNKS,)),
            pltpu.SemaphoreType.DMA((12,)),
            pltpu.SemaphoreType.DMA((12,)),
            pltpu.SemaphoreType.DMA((2, peers)),
            pltpu.SemaphoreType.DMA((2, peers)),
            pltpu.SemaphoreType.DMA((2, NY * NC - 1)),
        ],
        compiler_params=pltpu.CompilerParams(
            collective_id=0, has_side_effects=True, vmem_limit_bytes=40 * 1024 * 1024),
    )(normed_input, gate_cotangent, first_value_cot, second_value_cot, head_lambda, projection,
      gate_weight, value_weight, gate_first, gate_second, value_first, value_second)
    shape = jax.ShapeDtypeStruct
    return pl.pallas_call(
        finish_kernel,
        name="finish",
        in_specs=[vmem] * 10,
        out_specs=[vmem, vmem, hbm, vmem, vmem, vmem, vmem, hbm, vmem, vmem],
        out_shape=[
            shape((ROWS, GATE), f32), shape((ROWS, GATE), f32), shape((D, GATE), bf16),
            shape((OWN, GATE), f32), shape((OWN, GATE), f32),
            shape((ROWS, VALUE), f32), shape((ROWS, VALUE), f32), shape((D, VALUE), bf16),
            shape((OWN, VALUE), f32), shape((OWN, VALUE), f32),
        ],
        scratch_shapes=[
            pltpu.VMEM((D, GATE), bf16), pltpu.VMEM((D, VALUE), bf16), pltpu.SemaphoreType.DMA((8,)),
        ],
        compiler_params=pltpu.CompilerParams(vmem_limit_bytes=24 * 1024 * 1024),
    )(low, upd, wall, tot, gate_weight, value_weight, gate_first, gate_second, value_first, value_second)


def solution(mesh):
    torus = Mesh(mesh.devices.reshape(NZ, NX, NY, NC), AXES)
    split = P(FS, TP)
    return jax.shard_map(
        per_device,
        mesh=torus,
        in_specs=(P(FS, None), split, split, split, P(TP), P(), split, split, split, split, split, split),
        out_specs=(split, split, P(None, TP), split, split, split, split, P(None, TP), split, split),
        check_vma=False,
    )
```

time: 219 us -> 60.8 us (0.28)
  the two profiles are of different devices: /device:TPU:1 before, /device:TPU:16 now
where the time goes in v1:
time: 60.8 us; the launch traced here: 60.3 us
  Pallas kernels  50.1 us (82%)
  local copies, waits for them, and re-layouts  8.89 us (15%)
  between operations  1.32 us (2%)
    pallas_call x1, Pallas kernels, per_device(): pl.pallas_call(exchange_kernel, name='exchange', in_specs=[hbm, hbm, hbm,...  47.9 us
    unnamed x20, local copies, waits for them, and re-layouts  8.89 us
    pallas_call x1, Pallas kernels, per_device(): pl.pallas_call(finish_kernel, name='finish', in_specs=[vmem] * 10, out_sp...  2.18 us

profile of v1, /device:TPU:16, one launch (start us, length us, event | category | flops | bytes accessed | tf_op | source)
XLA Modules:
  0.0 60.3 jit_solution(17130379105980411694)
XLA Ops:
  1.3 0.0 copy-start
  1.3 1.2 %copy-done = bf16[2048,256]{1,0:T(8,128)(2,1)S(1)} copy-done((bf16[2048,256]{1,0:T(8,128)(2,1)S(1)}, bf16[2048,256]{1,0:T(8,128)(2,1)}, u32[]{:S(2)}) %copy-start) | copy-done | bytes 1048600
  2.5 0.0 copy-start.1
  2.5 1.2 %copy-done.1 = bf16[2048,256]{1,0:T(8,128)(2,1)S(1)} copy-done((bf16[2048,256]{1,0:T(8,128)(2,1)S(1)}, bf16[2048,256]{1,0:T(8,128)(2,1)}, u32[]{:S(2)}) %copy-start.1) | copy-done | bytes 1048600
  3.7 0.0 copy-start.2
  3.7 1.0 %copy-done.2 = bf16[2048,128]{1,0:T(8,128)(2,1)S(1)} copy-done((bf16[2048,128]{1,0:T(8,128)(2,1)S(1)}, bf16[2048,128]{1,0:T(8,128)(2,1)}, u32[]{:S(2)}) %copy-start.2) | copy-done | bytes 524312
  4.8 0.0 copy-start.3
  4.8 1.0 %copy-done.3 = bf16[2048,128]{1,0:T(8,128)(2,1)S(1)} copy-done((bf16[2048,128]{1,0:T(8,128)(2,1)S(1)}, bf16[2048,128]{1,0:T(8,128)(2,1)}, u32[]{:S(2)}) %copy-start.3) | copy-done | bytes 524312
  5.8 0.0 copy-start.4
  5.8 0.8 %copy-done.4 = f32[64,256]{1,0:T(8,128)S(1)} copy-done((f32[64,256]{1,0:T(8,128)S(1)}, f32[64,256]{1,0:T(8,128)}, u32[]{:S(2)}) %copy-start.4) | copy-done | bytes 65560
  6.7 0.0 copy-start.5
  6.7 0.8 %copy-done.5 = f32[64,128]{1,0:T(8,128)S(1)} copy-done((f32[64,128]{1,0:T(8,128)S(1)}, f32[64,128]{1,0:T(8,128)}, u32[]{:S(2)}) %copy-start.5) | copy-done | bytes 32792
  7.4 0.0 copy-start.6
  7.4 0.7 %copy-done.6 = f32[8,256]{1,0:T(8,128)S(1)} copy-done((f32[8,256]{1,0:T(8,128)S(1)}, f32[8,256]{1,0:T(8,128)}, u32[]{:S(2)}) %copy-start.6) | copy-done | bytes 8216
  8.1 0.0 copy-start.7
  8.1 0.7 %copy-done.7 = f32[8,256]{1,0:T(8,128)S(1)} copy-done((f32[8,256]{1,0:T(8,128)S(1)}, f32[8,256]{1,0:T(8,128)}, u32[]{:S(2)}) %copy-start.7) | copy-done | bytes 8216
  8.8 0.0 copy-start.8
  8.8 0.7 %copy-done.8 = f32[8,128]{1,0:T(8,128)S(1)} copy-done((f32[8,128]{1,0:T(8,128)S(1)}, f32[8,128]{1,0:T(8,128)}, u32[]{:S(2)}) %copy-start.8) | copy-done | bytes 4120
  9.5 0.0 copy-start.9
  9.5 0.7 %copy-done.9 = f32[8,128]{1,0:T(8,128)S(1)} copy-done((f32[8,128]{1,0:T(8,128)S(1)}, f32[8,128]{1,0:T(8,128)}, u32[]{:S(2)}) %copy-start.9) | copy-done | bytes 4120
  10.2 47.9 %exchange.1 = (f32[8,384]{1,0:T(8,128)S(1)}, f32[2048,384]{1,0:T(8,128)S(1)}, bf16[4,8,64,384]{3,2,1,0:T(8,128)(2,1)S(1)}, f32[8,8,256]{2,1,0:T(8,128)S(1)}) custom-call(bf16[2048,2048]{1,0:T(8,128)(2,1)} %x_hbm.1, bf16[2048,256]{1,0:T(8,128)(2,1)S(1)} %copy-done, bf16[2048,128]{1,0:T(8,128)(2,1)S(1)} %copy-done.2, bf16[2048,128]{1,0:T(8,128)(2,1)S(1)} %copy-done.3, ...), custom_call_target="tpu_custom_call" | custom-call | tf_op jit(solution)/shard_map/exchange/pallas_call | solution.py:275
  58.1 2.2 %finish.1 = (f32[64,256]{1,0:T(8,128)}, f32[64,256]{1,0:T(8,128)}, bf16[2048,256]{1,0:T(8,128)(2,1)}, f32[8,256]{1,0:T(8,128)}, f32[8,256]{1,0:T(8,128)}, /*inde...) custom-call(f32[8,384]{1,0:T(8,128)S(1)} %get-tuple-element.14.low_ref,, ...), custom_call_target="tpu_custom_call" | custom-call | tf_op jit(solution)/shard_map/finish/pallas_call | solution.py:315
Async XLA Ops:
  1.3 1.2 %copy-start = (bf16[2048,256]{1,0:T(8,128)(2,1)S(1)}, bf16[2048,256]{1,0:T(8,128)(2,1)}, u32[]{:S(2)}) copy-start(bf16[2048,256]{1,0:T(8,128)(2,1)} %gate_hbm.1) | copy-start | bytes 3145732
  2.5 1.2 %copy-start.1 = (bf16[2048,256]{1,0:T(8,128)(2,1)S(1)}, bf16[2048,256]{1,0:T(8,128)(2,1)}, u32[]{:S(2)}) copy-start(bf16[2048,256]{1,0:T(8,128)(2,1)} %proj_hbm.1) | copy-start | bytes 3145732
  3.7 1.0 %copy-start.2 = (bf16[2048,128]{1,0:T(8,128)(2,1)S(1)}, bf16[2048,128]{1,0:T(8,128)(2,1)}, u32[]{:S(2)}) copy-start(bf16[2048,128]{1,0:T(8,128)(2,1)} %one_hbm.1) | copy-start | bytes 1572868
  4.8 1.0 %copy-start.3 = (bf16[2048,128]{1,0:T(8,128)(2,1)S(1)}, bf16[2048,128]{1,0:T(8,128)(2,1)}, u32[]{:S(2)}) copy-start(bf16[2048,128]{1,0:T(8,128)(2,1)} %two_hbm.1) | copy-start | bytes 1572868
  5.8 0.8 %copy-start.4 = (f32[64,256]{1,0:T(8,128)S(1)}, f32[64,256]{1,0:T(8,128)}, u32[]{:S(2)}) copy-start(f32[64,256]{1,0:T(8,128)} %gw_ref.1) | copy-start | bytes 196612
  6.7 0.8 %copy-start.5 = (f32[64,128]{1,0:T(8,128)S(1)}, f32[64,128]{1,0:T(8,128)}, u32[]{:S(2)}) copy-start(f32[64,128]{1,0:T(8,128)} %vw_ref.1) | copy-start | bytes 98308
  7.4 0.7 %copy-start.6 = (f32[8,256]{1,0:T(8,128)S(1)}, f32[8,256]{1,0:T(8,128)}, u32[]{:S(2)}) copy-start(f32[8,256]{1,0:T(8,128)} %gf_ref.1) | copy-start | bytes 24580
  8.1 0.7 %copy-start.7 = (f32[8,256]{1,0:T(8,128)S(1)}, f32[8,256]{1,0:T(8,128)}, u32[]{:S(2)}) copy-start(f32[8,256]{1,0:T(8,128)} %gs_ref.1) | copy-start | bytes 24580
  8.8 0.7 %copy-start.8 = (f32[8,128]{1,0:T(8,128)S(1)}, f32[8,128]{1,0:T(8,128)}, u32[]{:S(2)}) copy-start(f32[8,128]{1,0:T(8,128)} %vf_ref.1) | copy-start | bytes 12292
  9.5 0.7 %copy-start.9 = (f32[8,128]{1,0:T(8,128)S(1)}, f32[8,128]{1,0:T(8,128)}, u32[]{:S(2)}) copy-start(f32[8,128]{1,0:T(8,128)} %vs_ref.1) | copy-start | bytes 12292

commit v2 on v1

--- a/solution.py
+++ b/solution.py
@@ -44,8 +44,8 @@
     x_hbm, gate_hbm, one_hbm, two_hbm, lam_ref, proj_hbm, gw_hbm, vw_hbm, gf_hbm, gs_hbm, vf_hbm, vs_hbm,
     low_ref, upd_ref, wall_ref, tot_ref,
     xbuf, gbuf, onebuf, twobuf, pbuf, gwbuf, vwbuf, gfbuf, gsbuf, vfbuf, vsbuf,
-    acc, part, landed, dirs,
-    in_sems, x_sems, w_send, w_recv, rs_sems, ag_sems, tot_sems,
+    ptbuf, acc, part, landed, dirs,
+    in_sems, x_sems, w_sems, rs_sems, ag_sems, tot_sems,
 ):
     z, x, y, c = [lax.axis_index(a) for a in AXES]
     me = z * NX + x
@@ -54,7 +54,9 @@
     def at(dz, dx):
         return (lax.rem(z + dz, NZ), lax.rem(x + dx, NX), y, c)
 
-    offsets = [(dz, dx) for dz in range(NZ) for dx in range(NX) if (dz, dx) != (0, 0)]
+    offsets = sorted(
+        [(dz, dx) for dz in range(NZ) for dx in range(NX) if (dz, dx) != (0, 0)],
+        key=lambda o: -(min(o[0], NZ - o[0]) + min(o[1], NX - o[1])))
     tp_offsets = [(dy, dc) for dy in range(NY) for dc in range(NC) if (dy, dc) != (0, 0)]
 
     def tp_at(dy, dc):
@@ -93,34 +95,66 @@
     wall_ref[x, z, :, 0:GATE] = gwbuf[...].astype(bf16)
     wall_ref[x, z, :, GATE:BOTH] = vwbuf[...].astype(bf16)
     loads[2].wait()
-
-    pl.semaphore_wait(barrier, len(offsets) + len(tp_offsets))
+    ptbuf[...] = pbuf[...].T
 
     def remote(src, dst, send, recv, device):
         return pltpu.make_async_remote_copy(
             src_ref=src, dst_ref=dst, send_sem=send, recv_sem=recv, device_id=device, device_id_type=MESH)
 
-    up, down = at(1, 0), at(NZ - 1, 0)
-    east, west = at(0, 1), at(0, NX - 1)
-    w_copies = []
-
-    def w_step(step):
-        pair = []
-        for way, device in ((0, up), (1, down)):
-            slot = lax.rem(z + (NZ - step if way == 0 else step), NZ)
-            block = wall_ref.at[x, slot]
-            if step == NZ // 2 - 1:
-                block = block.at[pl.ds(way * (ROWS // 2), ROWS // 2)]
-            pair.append(remote(block, block, w_send.at[2 * step + way], w_recv.at[2 * step + way], device))
-        for copy in pair:
-            copy.start()
-        w_copies.append(pair)
-
-    def w_landed(step):
-        for copy in w_copies[step]:
+    w_sent = []
+
+    def w_copy(part, device):
+        n = len(w_sent)
+        copy = remote(part, part, w_sems.at[0, n], w_sems.at[1, n], device)
+        copy.start()
+        w_sent.append(copy)
+        return copy
+
+    def block(dz, dx=0):
+        return wall_ref.at[lax.rem(x + dx + NX, NX), lax.rem(z + dz + NZ, NZ)]
+
+    low_half, high_half = pl.ds(0, ROWS // 2), pl.ds(ROWS // 2, ROWS // 2)
+
+    def to(dz, dx=0):
+        return at(dz % NZ, dx % NX)
+
+    def landed_from(copies):
+        for copy in copies:
             copy.wait_recv()
 
-    w_step(0)
+    def beside(steps):
+        return [w_copy(block(dz), to(0, dx)) for dz in steps for dx in (1, -1)]
+
+    def across(steps):
+        return [w_copy(block(dz, -dx).at[half], to(0, dx)) for dz in steps for dx, half in ((1, low_half), (-1, high_half))]
+
+    near, far = (1, -1, 2, -2), (3, -3, 4)
+
+    w = {}
+
+    def w_start():
+        w["z1"] = [w_copy(block(0), to(dz)) for dz in near]
+        w["x0"] = beside((0,))
+
+    def w_middle():
+        landed_from(w["z1"])
+        w["z2"] = [
+            w_copy(block(-2), to(1)), w_copy(block(2), to(-1)),
+            w_copy(block(-2).at[low_half], to(2)), w_copy(block(2).at[high_half], to(-2)),
+        ]
+        w["x1"] = beside(near)
+        landed_from(w["x0"])
+        w["f0"] = across((0,))
+
+    def w_late():
+        landed_from(w["z2"])
+        w["x2"] = beside(far)
+        landed_from(w["x1"])
+        w["f1"] = across(near)
+
+    def w_last():
+        landed_from(w["x2"])
+        w["f2"] = across(far)
 
     def chunk(i):
         x_loads[i].wait()
@@ -128,25 +162,21 @@
             for copy in loads[3:6]:
                 copy.wait()
         rows = pl.ds(i * CHUNK, CHUNK)
-        projected = jnp.dot(xbuf[rows, :], pbuf[...], preferred_element_type=f32).astype(bf16)
+        projected = lax.dot_general(
+            ptbuf[...], xbuf[rows, :], (((1,), (1,)), ((), ())), preferred_element_type=f32).astype(bf16)
         value_cot = (onebuf[rows, :].astype(f32) - lam_ref[0] * twobuf[rows, :].astype(f32)).astype(bf16)
         both = jnp.concatenate([gbuf[rows, :], value_cot], axis=1)
-        term = lax.dot_general(projected, both, (((0,), (0,)), ((), ())), preferred_element_type=f32)
+        term = jnp.dot(projected, both, preferred_element_type=f32)
         if i == 0:
             acc[...] = term
         else:
             acc[...] += term
 
-    chunk(0)
-    w_landed(0)
-    w_step(1)
-    chunk(1)
-    w_landed(1)
-    w_step(2)
-    chunk(2)
-    w_landed(2)
-    w_step(3)
-    chunk(3)
+    for i in range(CHUNKS - 1):
+        chunk(i)
+    pl.semaphore_wait(barrier, len(offsets) + len(tp_offsets))
+    w_start()
+    chunk(CHUNKS - 1)
 
     part[...] = acc[...].reshape(NZ * NX, OWN, BOTH).astype(bf16)
     rs_copies = []
@@ -159,13 +189,7 @@
         copy.wait()
     landed[me] = part[me]
 
-    w_landed(3)
-    column = wall_ref.at[x]
-    x_copies = [
-        remote(column, column, w_send.at[8], w_recv.at[8], east),
-        remote(column, column, w_send.at[9], w_recv.at[9], west),
-    ]
-
+    w_middle()
     for copy in rs_copies:
         copy.wait_recv()
     low = jnp.sum(landed[...].astype(f32), axis=0)
@@ -178,8 +202,7 @@
     for j, (dz, dx) in enumerate(offsets):
         ag_copies.append(remote(dirs.at[me], dirs.at[me], ag_sems.at[0, j], ag_sems.at[1, j], at(dz, dx)))
         ag_copies[-1].start()
-    for copy in x_copies:
-        copy.start()
+    w_late()
     for copy in ag_copies:
         copy.wait_recv()
 
@@ -193,33 +216,20 @@
         squares = (update * update).reshape(64, 8, BOTH).sum(axis=0)
         gate_sum += squares[:, 0:128] + squares[:, 128:256]
         value_sum += squares[:, 256:384]
-    tot_ref[my_tp, :, 0:128] = gate_sum
-    tot_ref[my_tp, :, 128:256] = value_sum
+    tot_ref[my_tp, 0:4, :] = gate_sum[0:4] + gate_sum[4:8]
+    tot_ref[my_tp, 4:8, :] = value_sum[0:4] + value_sum[4:8]
     tot_copies = []
     for j, (dy, dc) in enumerate(tp_offsets):
         tot_copies.append(
             remote(tot_ref.at[my_tp], tot_ref.at[my_tp], tot_sems.at[0, j], tot_sems.at[1, j], tp_at(dy, dc)))
         tot_copies[-1].start()
 
-    for copy in x_copies:
-        copy.wait_recv()
-    half = NZ // 2
-    from_west = wall_ref.at[lax.rem(x + NX - 1, NX), pl.ds(0, half)]
-    from_east = wall_ref.at[lax.rem(x + 1, NX), pl.ds(half, half)]
-    far_copies = [
-        remote(from_west, from_west, w_send.at[10], w_recv.at[10], east),
-        remote(from_east, from_east, w_send.at[11], w_recv.at[11], west),
-    ]
-    for copy in far_copies:
-        copy.start()
+    w_last()
     for copy in tot_copies:
         copy.wait_recv()
-    for copy in far_copies:
-        copy.wait_recv()
-    for pair in w_copies:
-        for copy in pair:
-            copy.wait_send()
-    for copy in rs_copies + ag_copies + x_copies + far_copies + tot_copies:
+    for name in ("f0", "f1", "f2"):
+        landed_from(w[name])
+    for copy in w_sent + rs_copies + ag_copies + tot_copies:
         copy.wait_send()
 
 
@@ -230,9 +240,9 @@
 ):
     z, x = lax.axis_index("z"), lax.axis_index("x")
     first_row = (z * NX + x) * ROWS
-    totals = jnp.sum(tot_ref[...], axis=(0, 1))
-    gate_total = jnp.sum(totals[0:128])
-    value_total = jnp.sum(totals[128:256])
+    totals = jnp.sum(tot_ref[...], axis=0)
+    gate_total = jnp.sum(totals[0:4])
+    value_total = jnp.sum(totals[4:8])
     gate_scale = 1.0 / (jnp.sqrt(jnp.full((8, 128), gate_total, f32) / (D * D)) + rms_floor)
     value_scale = 1.0 / (jnp.sqrt(jnp.full((8, 128), value_total, f32) / (D * 8 * VALUE)) + rms_floor)
     gate_scale = jnp.max(gate_scale)
@@ -281,7 +291,7 @@
             jax.ShapeDtypeStruct((OWN, BOTH), f32),
             jax.ShapeDtypeStruct((D, BOTH), f32),
             jax.ShapeDtypeStruct((NX, NZ, ROWS, BOTH), bf16),
-            jax.ShapeDtypeStruct((NY * NC, 8, 256), f32),
+            jax.ShapeDtypeStruct((NY * NC, 8, 128), f32),
         ],
         scratch_shapes=[
             pltpu.VMEM((TOKENS, D), bf16),
@@ -295,22 +305,24 @@
             pltpu.VMEM((OWN, GATE), f32),
             pltpu.VMEM((OWN, VALUE), f32),
             pltpu.VMEM((OWN, VALUE), f32),
+            pltpu.VMEM((RANK, D), bf16),
             pltpu.VMEM((RANK, BOTH), f32),
             pltpu.VMEM((NZ * NX, OWN, BOTH), bf16),
             pltpu.VMEM((NZ * NX, OWN, BOTH), bf16),
             pltpu.VMEM((NZ * NX, OWN, BOTH), bf16),
             pltpu.SemaphoreType.DMA((10,)),
             pltpu.SemaphoreType.DMA((CHUNKS,)),
-            pltpu.SemaphoreType.DMA((12,)),
-            pltpu.SemaphoreType.DMA((12,)),
+            pltpu.SemaphoreType.DMA((2, 42)),
             pltpu.SemaphoreType.DMA((2, peers)),
             pltpu.SemaphoreType.DMA((2, peers)),
             pltpu.SemaphoreType.DMA((2, NY * NC - 1)),
         ],
         compiler_params=pltpu.CompilerParams(
             collective_id=0, has_side_effects=True, vmem_limit_bytes=40 * 1024 * 1024),
-    )(normed_input, gate_cotangent, first_value_cot, second_value_cot, head_lambda, projection,
-      gate_weight, value_weight, gate_first, gate_second, value_first, value_second)
+    )(*[pltpu.with_memory_space_constraint(a, pltpu.HBM) for a in (normed_input, gate_cotangent, first_value_cot, second_value_cot)],
+      head_lambda,
+      *[pltpu.with_memory_space_constraint(a, pltpu.HBM) for a in (
+          projection, gate_weight, value_weight, gate_first, gate_second, value_first, value_second)])
     shape = jax.ShapeDtypeStruct
     return pl.pallas_call(
         finish_kernel,

time: 60.8 us -> 40.6 us (0.67)
  the two profiles are of different devices: /device:TPU:16 before, /device:TPU:1 now
where the time goes in v2:
time: 40.6 us
  Pallas kernels  39.1 us (96%)
  between operations  1.39 us (3%)
    pallas_call x1, Pallas kernels, per_device(): pl.pallas_call(exchange_kernel, name='exchange', in_specs=[hbm, hbm, hbm,...  37 us
    pallas_call x1, Pallas kernels, per_device(): pl.pallas_call(finish_kernel, name='finish', in_specs=[vmem] * 10, out_sp...  2.17 us

profile of v2, /device:TPU:1, one launch (start us, length us, event | category | flops | bytes accessed | tf_op | source)
XLA Modules:
  0.0 40.6 jit_solution(3849708588559091926)
XLA Ops:
  1.3 0.0 copy-start
  1.3 0.0 copy-start.1
  1.3 0.0 copy-start.2
  1.3 0.0 copy-start.3
  1.3 0.0 copy-start.4
  1.3 0.0 copy-start.5
  1.4 37.0 %exchange.1 = (f32[8,384]{1,0:T(8,128)S(1)}, f32[2048,384]{1,0:T(8,128)S(1)}, bf16[4,8,64,384]{3,2,1,0:T(8,128)(2,1)S(1)}, f32[8,8,128]{2,1,0:T(8,128)S(1)}) custom-call(bf16[2048,2048]{1,0:T(8,128)(2,1)} %x_hbm.1, bf16[2048,256]{1,0:T(8,128)(2,1)} %gate_hbm.1, bf16[2048,128]{1,0:T(8,128)(2,1)} %one_hbm.1, bf16[2048,128]{1,0:T(8,128)(2,1)} %two_hbm.1, ...), custom_call_target="tpu_custom_call" | custom-call | tf_op jit(solution)/shard_map/exchange/pallas_call | solution.py:285
  38.3 0.0 copy-done
  38.3 0.0 copy-done.1
  38.3 0.0 copy-done.2
  38.4 0.0 copy-done.3
  38.4 0.0 copy-done.4
  38.4 0.0 copy-done.5
  38.4 2.2 %finish.1 = (f32[64,256]{1,0:T(8,128)}, f32[64,256]{1,0:T(8,128)}, bf16[2048,256]{1,0:T(8,128)(2,1)}, f32[8,256]{1,0:T(8,128)}, f32[8,256]{1,0:T(8,128)}, /*inde...) custom-call(f32[8,384]{1,0:T(8,128)S(1)} %get-tuple-element.14.low_ref,, ...), custom_call_target="tpu_custom_call" | custom-call | tf_op jit(solution)/shard_map/finish/pallas_call | solution.py:327
Async XLA Ops:
  1.3 37.0 %copy-start = (f32[64,256]{1,0:T(8,128)S(1)}, f32[64,256]{1,0:T(8,128)}, u32[]{:S(2)}) copy-start(f32[64,256]{1,0:T(8,128)} %gw_ref.1) | copy-start | bytes 196612
  1.3 37.0 %copy-start.1 = (f32[64,128]{1,0:T(8,128)S(1)}, f32[64,128]{1,0:T(8,128)}, u32[]{:S(2)}) copy-start(f32[64,128]{1,0:T(8,128)} %vw_ref.1) | copy-start | bytes 98308
  1.3 37.0 %copy-start.2 = (f32[8,256]{1,0:T(8,128)S(1)}, f32[8,256]{1,0:T(8,128)}, u32[]{:S(2)}) copy-start(f32[8,256]{1,0:T(8,128)} %gf_ref.1) | copy-start | bytes 24580
  1.3 37.0 %copy-start.3 = (f32[8,256]{1,0:T(8,128)S(1)}, f32[8,256]{1,0:T(8,128)}, u32[]{:S(2)}) copy-start(f32[8,256]{1,0:T(8,128)} %gs_ref.1) | copy-start | bytes 24580
  1.3 37.0 %copy-start.4 = (f32[8,128]{1,0:T(8,128)S(1)}, f32[8,128]{1,0:T(8,128)}, u32[]{:S(2)}) copy-start(f32[8,128]{1,0:T(8,128)} %vf_ref.1) | copy-start | bytes 12292
  1.3 37.0 %copy-start.5 = (f32[8,128]{1,0:T(8,128)S(1)}, f32[8,128]{1,0:T(8,128)}, u32[]{:S(2)}) copy-start(f32[8,128]{1,0:T(8,128)} %vs_ref.1) | copy-start | bytes 12292

commit v3 on v2

v3 whole, which is shorter than its diff:
```python
import functools

import jax
import jax.numpy as jnp
from jax import lax
from jax.experimental import pallas as pl
from jax.experimental.pallas import tpu as pltpu
from jax.sharding import Mesh
from jax.sharding import PartitionSpec as P

D = 2048
RANK = 256
GATE = 256
VALUE = 128
BOTH = GATE + VALUE
NZ, NX, NY, NC = 8, 4, 4, 2
FS = ("z", "x")
TP = ("y", "c")
AXES = ("z", "x", "y", "c")
OWN = RANK // (NZ * NX)
ROWS = D // (NZ * NX)
TOKENS = 2048
CHUNKS = 4
CHUNK = TOKENS // CHUNKS

moment_decay = 0.9
square_decay = 0.95
adam_floor = 1e-08
learn_rate = 0.02
rms_floor = 0.1

MESH = pl.DeviceIdType.MESH
f32 = jnp.float32
bf16 = jnp.bfloat16


def moments(first, second, low):
    new_first = moment_decay * first + (1.0 - moment_decay) * low
    new_second = square_decay * second + (1.0 - square_decay) * low * low
    return new_first, new_second


def exchange_kernel(
    x_hbm, gate_hbm, one_hbm, two_hbm, lam_ref, proj_hbm, gw_hbm, vw_hbm, gf_hbm, gs_hbm, vf_hbm, vs_hbm,
    low_ref, upd_ref, wall_ref, tot_ref,
    xbuf, gbuf, onebuf, twobuf, pbuf, gwbuf, vwbuf, gfbuf, gsbuf, vfbuf, vsbuf,
    ptbuf, acc, part, landed, dirs,
    in_sems, w_sems, rs_sems, ag_sems, tot_sems,
):
    z, x, y, c = [lax.axis_index(a) for a in AXES]
    me = z * NX + x
    my_tp = y * NC + c
    peers, tp_peers = NZ * NX - 1, NY * NC - 1

    def at(dz, dx):
        return (lax.rem(z + dz, NZ), lax.rem(x + dx, NX), y, c)

    offsets = sorted(
        [(dz, dx) for dz in range(NZ) for dx in range(NX) if (dz, dx) != (0, 0)],
        key=lambda o: -(min(o[0], NZ - o[0]) + min(o[1], NX - o[1])))
    tp_offsets = [(dy, dc) for dy in range(NY) for dc in range(NC) if (dy, dc) != (0, 0)]

    def tp_at(dy, dc):
        return (z, x, lax.rem(y + dy, NY), lax.rem(c + dc, NC))

    def load(src, dst, n):
        pltpu.make_async_copy(src, dst, in_sems.at[n]).start()

    def take(sem, amount):
        pltpu.make_async_copy(amount, amount, sem).wait()

    def load_x(i):
        rows = pl.ds(i * CHUNK, CHUNK)
        load(x_hbm.at[rows], xbuf.at[rows], 4 + i)

    load(proj_hbm, pbuf, 0)
    load(gw_hbm, gwbuf, 1)
    load(vw_hbm, vwbuf, 1)
    load_x(0)

    barrier = pltpu.get_barrier_semaphore()
    for dz, dx in offsets:
        pl.semaphore_signal(barrier, inc=1, device_id=at(dz, dx), device_id_type=MESH)
    for dy, dc in tp_offsets:
        pl.semaphore_signal(barrier, inc=1, device_id=tp_at(dy, dc), device_id_type=MESH)

    load_x(1)
    take(in_sems.at[1], acc.at[pl.ds(0, 64)])
    wall_ref[x, z, :, 0:GATE] = gwbuf[...].astype(bf16)
    wall_ref[x, z, :, GATE:BOTH] = vwbuf[...].astype(bf16)
    take(in_sems.at[0], pbuf)
    load(gate_hbm, gbuf, 2)
    load(one_hbm, onebuf, 2)
    load(two_hbm, twobuf, 2)
    load_x(2)
    ptbuf[...] = pbuf[...].T

    def remote(src, dst, send, recv, device):
        return pltpu.make_async_remote_copy(
            src_ref=src, dst_ref=dst, send_sem=send, recv_sem=recv, device_id=device, device_id_type=MESH)

    def w_copy(part, device, group):
        remote(part, part, w_sems.at[0, group], w_sems.at[1, group], device).start()

    def w_blocks(group, blocks, way):
        take(w_sems.at[way, group], wall_ref.at[0, pl.ds(0, blocks)])

    def block(dz, dx=0):
        return wall_ref.at[lax.rem(x + dx + NX, NX), lax.rem(z + dz + NZ, NZ)]

    low_half, high_half = pl.ds(0, ROWS // 2), pl.ds(ROWS // 2, ROWS // 2)

    def to(dz, dx=0):
        return at(dz % NZ, dx % NX)

    def beside(steps, group):
        for dz in steps:
            for dx in (1, -1):
                w_copy(block(dz), to(0, dx), group)

    def across(steps):
        for dz in steps:
            for dx, half in ((1, low_half), (-1, high_half)):
                w_copy(block(dz, -dx).at[half], to(0, dx), 5)

    near, far = (1, -1, 2, -2), (3, -3, 4)

    group_blocks = (4, 2, 3, 8, 6, 8)

    def w_start():
        for dz in near:
            w_copy(block(0), to(dz), 0)
        beside((0,), 1)

    def w_middle():
        w_blocks(0, 4, 1)
        w_copy(block(-2), to(1), 2)
        w_copy(block(2), to(-1), 2)
        w_copy(block(-2).at[low_half], to(2), 2)
        w_copy(block(2).at[high_half], to(-2), 2)
        beside(near, 3)
        w_blocks(1, 2, 1)
        across((0,))

    def w_late():
        w_blocks(2, 3, 1)
        beside(far, 4)
        w_blocks(3, 8, 1)
        across(near)

    def w_last():
        w_blocks(4, 6, 1)
        across(far)

    def second(i, projected):
        rows = pl.ds(i * CHUNK, CHUNK)
        value_cot = (onebuf[rows, :].astype(f32) - lam_ref[0] * twobuf[rows, :].astype(f32)).astype(bf16)
        both = jnp.concatenate([gbuf[rows, :], value_cot], axis=1)
        term = jnp.dot(projected, both, preferred_element_type=f32)
        if i == 0:
            acc[...] = term
        else:
            acc[...] += term

    def chunk(i):
        rows = pl.ds(i * CHUNK, CHUNK)
        take(in_sems.at[4 + i], xbuf.at[rows])
        if i == 0:
            load_x(3)
            load(gf_hbm, gfbuf, 3)
            load(gs_hbm, gsbuf, 3)
            load(vf_hbm, vfbuf, 3)
            load(vs_hbm, vsbuf, 3)
        if i == 1:
            take(in_sems.at[2], xbuf.at[pl.ds(0, 512)])
        if i > 0:
            second(i - 1, held[0])
        held[0] = lax.dot_general(
            ptbuf[...], xbuf[rows, :], (((1,), (1,)), ((), ())), preferred_element_type=f32).astype(bf16)

    held = [None]
    for i in range(CHUNKS - 1):
        chunk(i)
    pl.semaphore_wait(barrier, len(offsets) + len(tp_offsets))
    w_start()
    chunk(CHUNKS - 1)
    second(CHUNKS - 1, held[0])

    part[...] = acc[...].reshape(NZ * NX, OWN, BOTH).astype(bf16)
    for dz, dx in offsets:
        device = at(dz, dx)
        owner = device[0] * NX + device[1]
        remote(part.at[owner], landed.at[me], rs_sems.at[0], rs_sems.at[1], device).start()
    take(in_sems.at[3], acc.at[pl.ds(0, 16)])
    landed[me] = part[me]

    w_middle()
    take(rs_sems.at[1], landed.at[pl.ds(0, peers)])
    low = jnp.sum(landed[...].astype(f32), axis=0)
    low_ref[...] = low
    gate_first, gate_second = moments(gfbuf[...], gsbuf[...], low[:, 0:GATE])
    value_first, value_second = moments(vfbuf[...], vsbuf[...], low[:, GATE:BOTH])
    dirs[me, :, 0:GATE] = (gate_first / (jnp.sqrt(gate_second) + adam_floor)).astype(bf16)
    dirs[me, :, GATE:BOTH] = (value_first / (jnp.sqrt(value_second) + adam_floor)).astype(bf16)
    for dz, dx in offsets:
        remote(dirs.at[me], dirs.at[me], ag_sems.at[0], ag_sems.at[1], at(dz, dx)).start()
    w_late()
    take(ag_sems.at[1], dirs.at[pl.ds(0, peers)])

    spread = dirs[...].astype(f32).reshape(RANK, BOTH).astype(bf16)
    gate_sum = jnp.zeros((8, 128), f32)
    value_sum = jnp.zeros((8, 128), f32)
    for i in range(4):
        rows = pl.ds(i * 512, 512)
        update = jnp.dot(pbuf[rows, :], spread, preferred_element_type=f32)
        upd_ref[rows, :] = update
        squares = (update * update).reshape(64, 8, BOTH).sum(axis=0)
        gate_sum += squares[:, 0:128] + squares[:, 128:256]
        value_sum += squares[:, 256:384]
    tot_ref[my_tp, 0:4, :] = gate_sum[0:4] + gate_sum[4:8]
    tot_ref[my_tp, 4:8, :] = value_sum[0:4] + value_sum[4:8]
    for dy, dc in tp_offsets:
        remote(tot_ref.at[my_tp], tot_ref.at[my_tp], tot_sems.at[0], tot_sems.at[1], tp_at(dy, dc)).start()

    w_last()
    take(tot_sems.at[1], tot_ref.at[pl.ds(0, tp_peers)])
    w_blocks(5, 8, 1)
    for group, blocks in enumerate(group_blocks):
        w_blocks(group, blocks, 0)
    take(rs_sems.at[0], part.at[pl.ds(0, peers)])
    take(ag_sems.at[0], dirs.at[pl.ds(0, peers)])
    take(tot_sems.at[0], tot_ref.at[pl.ds(0, tp_peers)])


def finish_kernel(
    low_ref, upd_ref, wall_ref, tot_ref, gw_ref, vw_ref, gf_ref, gs_ref, vf_ref, vs_ref,
    ngw_hbm, gstep_hbm, gcopy_hbm, ngf_hbm, ngs_hbm, nvw_hbm, vstep_hbm, vcopy_hbm, nvf_hbm, nvs_hbm,
    ngw, gstep, gout, ngf, ngs, nvw, vstep, vout, nvf, nvs, sems,
):
    z, x = lax.axis_index("z"), lax.axis_index("x")
    first_row = (z * NX + x) * ROWS
    totals = jnp.sum(tot_ref[...], axis=0)
    gate_total = jnp.sum(totals[0:4], keepdims=True)
    value_total = jnp.sum(totals[4:8], keepdims=True)
    gate_scale = 1.0 / (jnp.sqrt(gate_total / (D * D)) + rms_floor)
    value_scale = 1.0 / (jnp.sqrt(value_total / (D * 8 * VALUE)) + rms_floor)
    mine = upd_ref[pl.ds(pl.multiple_of(first_row, ROWS), ROWS), :]
    gate_step = mine[:, 0:GATE] * gate_scale
    value_step = mine[:, GATE:BOTH] * value_scale
    gstep[...] = gate_step
    vstep[...] = value_step
    ngw[...] = gw_ref[...] - learn_rate * gate_step
    nvw[...] = vw_ref[...] - learn_rate * value_step
    ngf[...], ngs[...] = moments(gf_ref[...], gs_ref[...], low_ref[:, 0:GATE])
    nvf[...], nvs[...] = moments(vf_ref[...], vs_ref[...], low_ref[:, GATE:BOTH])
    for src, dst in (
        (ngw, ngw_hbm), (gstep, gstep_hbm), (nvw, nvw_hbm), (vstep, vstep_hbm),
        (ngf, ngf_hbm), (ngs, ngs_hbm), (nvf, nvf_hbm), (nvs, nvs_hbm),
    ):
        pltpu.make_async_copy(src, dst, sems.at[0]).start()
    for f in range(NZ * NX):
        rows = pl.ds(f * ROWS, ROWS)
        update = upd_ref[rows, :]
        old = wall_ref[f % NX, f // NX].astype(f32)
        gout[rows, :] = (old[:, 0:GATE] - learn_rate * (update[:, 0:GATE] * gate_scale)).astype(bf16)
        vout[rows, :] = (old[:, GATE:BOTH] - learn_rate * (update[:, GATE:BOTH] * value_scale)).astype(bf16)
        if f % 4 == 3:
            span = pl.ds((f - 3) * ROWS, 4 * ROWS)
            pltpu.make_async_copy(gout.at[span], gcopy_hbm.at[span], sems.at[1]).start()
            pltpu.make_async_copy(vout.at[span], vcopy_hbm.at[span], sems.at[2]).start()
    small = upd_ref.at[pl.ds(0, 144)]
    pltpu.make_async_copy(small, small, sems.at[0]).wait()
    pltpu.make_async_copy(gout, gout, sems.at[1]).wait()
    pltpu.make_async_copy(vout, vout, sems.at[2]).wait()


def per_device(
    normed_input, gate_cotangent, first_value_cot, second_value_cot, head_lambda, projection,
    gate_weight, gate_first, gate_second, value_weight, value_first, value_second,
):
    hbm = pl.BlockSpec(memory_space=pltpu.HBM)
    vmem = pl.BlockSpec(memory_space=pltpu.VMEM)
    smem = pl.BlockSpec(memory_space=pltpu.SMEM)
    low, upd, wall, tot = pl.pallas_call(
        exchange_kernel,
        name="exchange",
        in_specs=[hbm, hbm, hbm, hbm, smem, hbm, hbm, hbm, hbm, hbm, hbm, hbm],
        out_specs=[vmem] * 4,
        out_shape=[
            jax.ShapeDtypeStruct((OWN, BOTH), f32),
            jax.ShapeDtypeStruct((D, BOTH), f32),
            jax.ShapeDtypeStruct((NX, NZ, ROWS, BOTH), bf16),
            jax.ShapeDtypeStruct((NY * NC, 8, 128), f32),
        ],
        scratch_shapes=[
            pltpu.VMEM((TOKENS, D), bf16),
            pltpu.VMEM((TOKENS, GATE), bf16),
            pltpu.VMEM((TOKENS, VALUE), bf16),
            pltpu.VMEM((TOKENS, VALUE), bf16),
            pltpu.VMEM((D, RANK), bf16),
            pltpu.VMEM((ROWS, GATE), f32),
            pltpu.VMEM((ROWS, VALUE), f32),
            pltpu.VMEM((OWN, GATE), f32),
            pltpu.VMEM((OWN, GATE), f32),
            pltpu.VMEM((OWN, VALUE), f32),
            pltpu.VMEM((OWN, VALUE), f32),
            pltpu.VMEM((RANK, D), bf16),
            pltpu.VMEM((RANK, BOTH), f32),
            pltpu.VMEM((NZ * NX, OWN, BOTH), bf16),
            pltpu.VMEM((NZ * NX, OWN, BOTH), bf16),
            pltpu.VMEM((NZ * NX, OWN, BOTH), bf16),
            pltpu.SemaphoreType.DMA((4 + CHUNKS,)),
            pltpu.SemaphoreType.DMA((2, 6)),
            pltpu.SemaphoreType.DMA((2,)),
            pltpu.SemaphoreType.DMA((2,)),
            pltpu.SemaphoreType.DMA((2,)),
        ],
        compiler_params=pltpu.CompilerParams(
            collective_id=0, has_side_effects=True, vmem_limit_bytes=40 * 1024 * 1024),
    )(*[a if a is head_lambda else pltpu.with_memory_space_constraint(a, pltpu.HBM) for a in (
        normed_input, gate_cotangent, first_value_cot, second_value_cot, head_lambda, projection,
        gate_weight, value_weight, gate_first, gate_second, value_first, value_second)])
    shape = jax.ShapeDtypeStruct
    outs = (
        ((ROWS, GATE), f32), ((ROWS, GATE), f32), ((D, GATE), bf16), ((OWN, GATE), f32), ((OWN, GATE), f32),
        ((ROWS, VALUE), f32), ((ROWS, VALUE), f32), ((D, VALUE), bf16), ((OWN, VALUE), f32), ((OWN, VALUE), f32),
    )
    return pl.pallas_call(
        finish_kernel,
        name="finish",
        in_specs=[vmem] * 10,
        out_specs=[hbm] * 10,
        out_shape=[shape(*o) for o in outs],
        scratch_shapes=[pltpu.VMEM(*o) for o in outs] + [pltpu.SemaphoreType.DMA((3,))],
        compiler_params=pltpu.CompilerParams(vmem_limit_bytes=24 * 1024 * 1024),
    )(low, upd, wall, tot, gate_weight, value_weight, gate_first, gate_second, value_first, value_second)


def solution(mesh):
    torus = Mesh(mesh.devices.reshape(NZ, NX, NY, NC), AXES)
    split = P(FS, TP)
    return jax.shard_map(
        per_device,
        mesh=torus,
        in_specs=(P(FS, None), split, split, split, P(TP), P(), split, split, split, split, split, split),
        out_specs=(split, split, P(None, TP), split, split, split, split, P(None, TP), split, split),
        check_vma=False,
    )
```

time: 40.6 us -> 37.1 us (0.914)
  Pallas kernels: 39.1 us -> 35.6 us
    pallas_call x1, Pallas kernels: 37 us -> 34.2 us  [per_device(): pl.pallas_call(exchange_kernel, name='exchange', in_specs=[hbm, hbm, hbm,...]
    pallas_call x1, Pallas kernels: 2.17 us -> 1.38 us  [per_device(): pl.pallas_call(finish_kernel, name='finish', in_specs=[vmem] * 10, out_sp...]
where the time goes in v3:
time: 37.1 us; the launch traced here: 37 us
  Pallas kernels  35.6 us (96%)
  between operations  1.39 us (4%)
    pallas_call x1, Pallas kernels, per_device(): pl.pallas_call(exchange_kernel, name='exchange', in_specs=[hbm, hbm, hbm,...  34.2 us
    pallas_call x1, Pallas kernels, per_device(): pl.pallas_call(finish_kernel, name='finish', in_specs=[vmem] * 10, out_sp...  1.38 us

profile of v3, /device:TPU:1, one launch (start us, length us, event | category | flops | bytes accessed | tf_op | source)
XLA Modules:
  0.0 37.0 jit_solution(12965832001543889423)
XLA Ops:
  1.3 0.0 copy-start
  1.3 0.0 copy-start.1
  1.3 0.0 copy-start.2
  1.3 0.0 copy-start.3
  1.3 0.0 copy-start.4
  1.3 0.0 copy-start.5
  1.4 34.2 %exchange.1 = (f32[8,384]{1,0:T(8,128)S(1)}, f32[2048,384]{1,0:T(8,128)S(1)}, bf16[4,8,64,384]{3,2,1,0:T(8,128)(2,1)S(1)}, f32[8,8,128]{2,1,0:T(8,128)S(1)}) custom-call(bf16[2048,2048]{1,0:T(8,128)(2,1)} %x_hbm.1, bf16[2048,256]{1,0:T(8,128)(2,1)} %gate_hbm.1, bf16[2048,128]{1,0:T(8,128)(2,1)} %one_hbm.1, bf16[2048,128]{1,0:T(8,128)(2,1)} %two_hbm.1, ...), custom_call_target="tpu_custom_call" | custom-call | tf_op jit(solution)/shard_map/exchange/pallas_call | solution.py:284
  35.6 0.0 copy-done
  35.6 0.0 copy-done.1
  35.6 0.0 copy-done.2
  35.6 0.0 copy-done.3
  35.6 0.0 copy-done.4
  35.6 0.0 copy-done.5
  35.6 1.4 %finish.1 = (f32[64,256]{1,0:T(8,128)}, f32[64,256]{1,0:T(8,128)}, bf16[2048,256]{1,0:T(8,128)(2,1)}, f32[8,256]{1,0:T(8,128)}, f32[8,256]{1,0:T(8,128)}, /*inde...) custom-call(f32[8,384]{1,0:T(8,128)S(1)} %get-tuple-element.14.low_ref,, ...), custom_call_target="tpu_custom_call" | custom-call | tf_op jit(solution)/shard_map/finish/pallas_call | solution.py:328
Async XLA Ops:
  1.3 34.3 %copy-start = (f32[64,256]{1,0:T(8,128)S(1)}, f32[64,256]{1,0:T(8,128)}, u32[]{:S(2)}) copy-start(f32[64,256]{1,0:T(8,128)} %gw_ref.1) | copy-start | bytes 196612
  1.3 34.3 %copy-start.1 = (f32[64,128]{1,0:T(8,128)S(1)}, f32[64,128]{1,0:T(8,128)}, u32[]{:S(2)}) copy-start(f32[64,128]{1,0:T(8,128)} %vw_ref.1) | copy-start | bytes 98308
  1.3 34.3 %copy-start.2 = (f32[8,256]{1,0:T(8,128)S(1)}, f32[8,256]{1,0:T(8,128)}, u32[]{:S(2)}) copy-start(f32[8,256]{1,0:T(8,128)} %gf_ref.1) | copy-start | bytes 24580
  1.3 34.3 %copy-start.3 = (f32[8,256]{1,0:T(8,128)S(1)}, f32[8,256]{1,0:T(8,128)}, u32[]{:S(2)}) copy-start(f32[8,256]{1,0:T(8,128)} %gs_ref.1) | copy-start | bytes 24580
  1.3 34.3 %copy-start.4 = (f32[8,128]{1,0:T(8,128)S(1)}, f32[8,128]{1,0:T(8,128)}, u32[]{:S(2)}) copy-start(f32[8,128]{1,0:T(8,128)} %vf_ref.1) | copy-start | bytes 12292
  1.3 34.3 %copy-start.5 = (f32[8,128]{1,0:T(8,128)S(1)}, f32[8,128]{1,0:T(8,128)}, u32[]{:S(2)}) copy-start(f32[8,128]{1,0:T(8,128)} %vs_ref.1) | copy-start | bytes 12292

commit v4 on v3

--- a/solution.py
+++ b/solution.py
@@ -133,14 +133,14 @@
         beside((0,), 1)
 
     def w_middle():
+        w_blocks(1, 2, 1)
+        across((0,))
         w_blocks(0, 4, 1)
         w_copy(block(-2), to(1), 2)
         w_copy(block(2), to(-1), 2)
         w_copy(block(-2).at[low_half], to(2), 2)
         w_copy(block(2).at[high_half], to(-2), 2)
         beside(near, 3)
-        w_blocks(1, 2, 1)
-        across((0,))
 
     def w_late():
         w_blocks(2, 3, 1)
@@ -179,11 +179,11 @@
             ptbuf[...], xbuf[rows, :], (((1,), (1,)), ((), ())), preferred_element_type=f32).astype(bf16)
 
     held = [None]
-    for i in range(CHUNKS - 1):
+    for i in range(CHUNKS):
+        if i == 1:
+            pl.semaphore_wait(barrier, len(offsets) + len(tp_offsets))
+            w_start()
         chunk(i)
-    pl.semaphore_wait(barrier, len(offsets) + len(tp_offsets))
-    w_start()
-    chunk(CHUNKS - 1)
     second(CHUNKS - 1, held[0])
 
     part[...] = acc[...].reshape(NZ * NX, OWN, BOTH).astype(bf16)

time: 37.1 us -> 36.4 us (0.981)
  Pallas kernels: 35.6 us -> 34.9 us
    pallas_call x1, Pallas kernels: 34.2 us -> 33.5 us  [per_device(): pl.pallas_call(exchange_kernel, name='exchange', in_specs=[hbm, hbm, hbm,...]
where the time goes in v4:
time: 36.4 us; the launch traced here: 36.3 us
  Pallas kernels  34.9 us (96%)
  between operations  1.39 us (4%)
    pallas_call x1, Pallas kernels, per_device(): pl.pallas_call(exchange_kernel, name='exchange', in_specs=[hbm, hbm, hbm,...  33.5 us
    pallas_call x1, Pallas kernels, per_device(): pl.pallas_call(finish_kernel, name='finish', in_specs=[vmem] * 10, out_sp...  1.38 us

profile of v4, /device:TPU:1, one launch (start us, length us, event | category | flops | bytes accessed | tf_op | source)
XLA Modules:
  0.0 36.3 jit_solution(13119940903729681388)
XLA Ops:
  1.3 0.0 copy-start
  1.3 0.0 copy-start.1
  1.3 0.0 copy-start.2
  1.3 0.0 copy-start.3
  1.3 0.0 copy-start.4
  1.3 0.0 copy-start.5
  1.4 33.5 %exchange.1 = (f32[8,384]{1,0:T(8,128)S(1)}, f32[2048,384]{1,0:T(8,128)S(1)}, bf16[4,8,64,384]{3,2,1,0:T(8,128)(2,1)S(1)}, f32[8,8,128]{2,1,0:T(8,128)S(1)}) custom-call(bf16[2048,2048]{1,0:T(8,128)(2,1)} %x_hbm.1, bf16[2048,256]{1,0:T(8,128)(2,1)} %gate_hbm.1, bf16[2048,128]{1,0:T(8,128)(2,1)} %one_hbm.1, bf16[2048,128]{1,0:T(8,128)(2,1)} %two_hbm.1, ...), custom_call_target="tpu_custom_call" | custom-call | tf_op jit(solution)/shard_map/exchange/pallas_call | solution.py:284
  34.9 0.0 copy-done
  34.9 0.0 copy-done.1
  34.9 0.0 copy-done.2
  34.9 0.0 copy-done.3
  34.9 0.0 copy-done.4
  34.9 0.0 copy-done.5
  34.9 1.4 %finish.1 = (f32[64,256]{1,0:T(8,128)}, f32[64,256]{1,0:T(8,128)}, bf16[2048,256]{1,0:T(8,128)(2,1)}, f32[8,256]{1,0:T(8,128)}, f32[8,256]{1,0:T(8,128)}, /*inde...) custom-call(f32[8,384]{1,0:T(8,128)S(1)} %get-tuple-element.14.low_ref,, ...), custom_call_target="tpu_custom_call" | custom-call | tf_op jit(solution)/shard_map/finish/pallas_call | solution.py:328
Async XLA Ops:
  1.3 33.6 %copy-start = (f32[64,256]{1,0:T(8,128)S(1)}, f32[64,256]{1,0:T(8,128)}, u32[]{:S(2)}) copy-start(f32[64,256]{1,0:T(8,128)} %gw_ref.1) | copy-start | bytes 196612
  1.3 33.6 %copy-start.1 = (f32[64,128]{1,0:T(8,128)S(1)}, f32[64,128]{1,0:T(8,128)}, u32[]{:S(2)}) copy-start(f32[64,128]{1,0:T(8,128)} %vw_ref.1) | copy-start | bytes 98308
  1.3 33.6 %copy-start.2 = (f32[8,256]{1,0:T(8,128)S(1)}, f32[8,256]{1,0:T(8,128)}, u32[]{:S(2)}) copy-start(f32[8,256]{1,0:T(8,128)} %gf_ref.1) | copy-start | bytes 24580
  1.3 33.6 %copy-start.3 = (f32[8,256]{1,0:T(8,128)S(1)}, f32[8,256]{1,0:T(8,128)}, u32[]{:S(2)}) copy-start(f32[8,256]{1,0:T(8,128)} %gs_ref.1) | copy-start | bytes 24580
  1.3 33.6 %copy-start.4 = (f32[8,128]{1,0:T(8,128)S(1)}, f32[8,128]{1,0:T(8,128)}, u32[]{:S(2)}) copy-start(f32[8,128]{1,0:T(8,128)} %vf_ref.1) | copy-start | bytes 12292
  1.3 33.6 %copy-start.5 = (f32[8,128]{1,0:T(8,128)S(1)}, f32[8,128]{1,0:T(8,128)}, u32[]{:S(2)}) copy-start(f32[8,128]{1,0:T(8,128)} %vs_ref.1) | copy-start | bytes 12292

commit v5 on v4

--- a/solution.py
+++ b/solution.py
@@ -44,7 +44,7 @@
     x_hbm, gate_hbm, one_hbm, two_hbm, lam_ref, proj_hbm, gw_hbm, vw_hbm, gf_hbm, gs_hbm, vf_hbm, vs_hbm,
     low_ref, upd_ref, wall_ref, tot_ref,
     xbuf, gbuf, onebuf, twobuf, pbuf, gwbuf, vwbuf, gfbuf, gsbuf, vfbuf, vsbuf,
-    ptbuf, acc, part, landed, dirs,
+    ptbuf, gram, acc, part, landed, dirs,
     in_sems, w_sems, rs_sems, ag_sems, tot_sems,
 ):
     z, x, y, c = [lax.axis_index(a) for a in AXES]
@@ -58,7 +58,9 @@
     offsets = sorted(
         [(dz, dx) for dz in range(NZ) for dx in range(NX) if (dz, dx) != (0, 0)],
         key=lambda o: -(min(o[0], NZ - o[0]) + min(o[1], NX - o[1])))
-    tp_offsets = [(dy, dc) for dy in range(NY) for dc in range(NC) if (dy, dc) != (0, 0)]
+    tp_offsets = sorted(
+        [(dy, dc) for dy in range(NY) for dc in range(NC) if (dy, dc) != (0, 0)],
+        key=lambda o: -(2 * min(o[0], NY - o[0]) + o[1]))
 
     def tp_at(dy, dc):
         return (z, x, lax.rem(y + dy, NY), lax.rem(c + dc, NC))
@@ -136,11 +138,11 @@
         w_blocks(1, 2, 1)
         across((0,))
         w_blocks(0, 4, 1)
+        beside(near, 3)
         w_copy(block(-2), to(1), 2)
         w_copy(block(2), to(-1), 2)
         w_copy(block(-2).at[low_half], to(2), 2)
         w_copy(block(2).at[high_half], to(-2), 2)
-        beside(near, 3)
 
     def w_late():
         w_blocks(2, 3, 1)
@@ -195,6 +197,11 @@
     landed[me] = part[me]
 
     w_middle()
+    products = lax.dot_general(ptbuf[...], pbuf[...], (((1,), (0,)), ((), ())), preferred_element_type=f32)
+    for term in range(3):
+        rounded = products.astype(bf16)
+        gram[pl.ds(term * RANK, RANK), :] = rounded
+        products = products - rounded.astype(f32)
     take(rs_sems.at[1], landed.at[pl.ds(0, peers)])
     low = jnp.sum(landed[...].astype(f32), axis=0)
     low_ref[...] = low
@@ -207,22 +214,22 @@
     w_late()
     take(ag_sems.at[1], dirs.at[pl.ds(0, peers)])
 
-    spread = dirs[...].astype(f32).reshape(RANK, BOTH).astype(bf16)
-    gate_sum = jnp.zeros((8, 128), f32)
-    value_sum = jnp.zeros((8, 128), f32)
-    for i in range(4):
-        rows = pl.ds(i * 512, 512)
-        update = jnp.dot(pbuf[rows, :], spread, preferred_element_type=f32)
-        upd_ref[rows, :] = update
-        squares = (update * update).reshape(64, 8, BOTH).sum(axis=0)
-        gate_sum += squares[:, 0:128] + squares[:, 128:256]
-        value_sum += squares[:, 256:384]
+    wide = dirs[...].astype(f32).reshape(RANK, BOTH)
+    spread = wide.astype(bf16)
+    terms = jnp.dot(gram[...], spread, preferred_element_type=f32)
+    terms = (terms[2 * RANK:] + terms[RANK:2 * RANK]) + terms[0:RANK]
+    squares = (wide * terms).reshape(RANK // 8, 8, BOTH).sum(axis=0)
+    gate_sum = squares[:, 0:128] + squares[:, 128:256]
+    value_sum = squares[:, 256:384]
     tot_ref[my_tp, 0:4, :] = gate_sum[0:4] + gate_sum[4:8]
     tot_ref[my_tp, 4:8, :] = value_sum[0:4] + value_sum[4:8]
     for dy, dc in tp_offsets:
         remote(tot_ref.at[my_tp], tot_ref.at[my_tp], tot_sems.at[0], tot_sems.at[1], tp_at(dy, dc)).start()
 
     w_last()
+    for i in range(4):
+        rows = pl.ds(i * 512, 512)
+        upd_ref[rows, :] = jnp.dot(pbuf[rows, :], spread, preferred_element_type=f32)
     take(tot_sems.at[1], tot_ref.at[pl.ds(0, tp_peers)])
     w_blocks(5, 8, 1)
     for group, blocks in enumerate(group_blocks):
@@ -240,8 +247,8 @@
     z, x = lax.axis_index("z"), lax.axis_index("x")
     first_row = (z * NX + x) * ROWS
     totals = jnp.sum(tot_ref[...], axis=0)
-    gate_total = jnp.sum(totals[0:4], keepdims=True)
-    value_total = jnp.sum(totals[4:8], keepdims=True)
+    gate_total = jnp.maximum(jnp.sum(totals[0:4], keepdims=True), 0.0)
+    value_total = jnp.maximum(jnp.sum(totals[4:8], keepdims=True), 0.0)
     gate_scale = 1.0 / (jnp.sqrt(gate_total / (D * D)) + rms_floor)
     value_scale = 1.0 / (jnp.sqrt(value_total / (D * 8 * VALUE)) + rms_floor)
     mine = upd_ref[pl.ds(pl.multiple_of(first_row, ROWS), ROWS), :]
@@ -305,6 +312,7 @@
             pltpu.VMEM((OWN, VALUE), f32),
             pltpu.VMEM((OWN, VALUE), f32),
             pltpu.VMEM((RANK, D), bf16),
+            pltpu.VMEM((3 * RANK, RANK), bf16),
             pltpu.VMEM((RANK, BOTH), f32),
             pltpu.VMEM((NZ * NX, OWN, BOTH), bf16),
             pltpu.VMEM((NZ * NX, OWN, BOTH), bf16),

time: 36.4 us -> 36 us (0.989)
  Pallas kernels: 34.9 us -> 34.5 us
    pallas_call x1, Pallas kernels: 33.5 us -> 33.1 us  [per_device(): pl.pallas_call(exchange_kernel, name='exchange', in_specs=[hbm, hbm, hbm,...]
where the time goes in v5:
time: 36 us; the launch traced here: 35.9 us
  Pallas kernels  34.5 us (96%)
  between operations  1.39 us (4%)
    pallas_call x1, Pallas kernels, per_device(): pl.pallas_call(exchange_kernel, name='exchange', in_specs=[hbm, hbm, hbm,...  33.1 us
    pallas_call x1, Pallas kernels, per_device(): pl.pallas_call(finish_kernel, name='finish', in_specs=[vmem] * 10, out_sp...  1.38 us

profile of v5, /device:TPU:1, one launch (start us, length us, event | category | flops | bytes accessed | tf_op | source)
XLA Modules:
  0.0 35.9 jit_solution(3825492669921171229)
XLA Ops:
  1.3 0.0 copy-start
  1.3 0.0 copy-start.1
  1.3 0.0 copy-start.2
  1.3 0.0 copy-start.3
  1.3 0.0 copy-start.4
  1.3 0.0 copy-start.5
  1.4 33.1 %exchange.1 = (f32[8,384]{1,0:T(8,128)S(1)}, f32[2048,384]{1,0:T(8,128)S(1)}, bf16[4,8,64,384]{3,2,1,0:T(8,128)(2,1)S(1)}, f32[8,8,128]{2,1,0:T(8,128)S(1)}) custom-call(bf16[2048,2048]{1,0:T(8,128)(2,1)} %x_hbm.1, bf16[2048,256]{1,0:T(8,128)(2,1)} %gate_hbm.1, bf16[2048,128]{1,0:T(8,128)(2,1)} %one_hbm.1, bf16[2048,128]{1,0:T(8,128)(2,1)} %two_hbm.1, ...), custom_call_target="tpu_custom_call" | custom-call | tf_op jit(solution)/shard_map/exchange/pallas_call | solution.py:291
  34.4 0.0 copy-done
  34.5 0.0 copy-done.1
  34.5 0.0 copy-done.2
  34.5 0.0 copy-done.3
  34.5 0.0 copy-done.4
  34.5 0.0 copy-done.5
  34.5 1.4 %finish.1 = (f32[64,256]{1,0:T(8,128)}, f32[64,256]{1,0:T(8,128)}, bf16[2048,256]{1,0:T(8,128)(2,1)}, f32[8,256]{1,0:T(8,128)}, f32[8,256]{1,0:T(8,128)}, /*inde...) custom-call(f32[8,384]{1,0:T(8,128)S(1)} %get-tuple-element.14.low_ref,, ...), custom_call_target="tpu_custom_call" | custom-call | tf_op jit(solution)/shard_map/finish/pallas_call | solution.py:336
Async XLA Ops:
  1.3 33.2 %copy-start = (f32[64,256]{1,0:T(8,128)S(1)}, f32[64,256]{1,0:T(8,128)}, u32[]{:S(2)}) copy-start(f32[64,256]{1,0:T(8,128)} %gw_ref.1) | copy-start | bytes 196612
  1.3 33.2 %copy-start.1 = (f32[64,128]{1,0:T(8,128)S(1)}, f32[64,128]{1,0:T(8,128)}, u32[]{:S(2)}) copy-start(f32[64,128]{1,0:T(8,128)} %vw_ref.1) | copy-start | bytes 98308
  1.3 33.2 %copy-start.2 = (f32[8,256]{1,0:T(8,128)S(1)}, f32[8,256]{1,0:T(8,128)}, u32[]{:S(2)}) copy-start(f32[8,256]{1,0:T(8,128)} %gf_ref.1) | copy-start | bytes 24580
  1.3 33.2 %copy-start.3 = (f32[8,256]{1,0:T(8,128)S(1)}, f32[8,256]{1,0:T(8,128)}, u32[]{:S(2)}) copy-start(f32[8,256]{1,0:T(8,128)} %gs_ref.1) | copy-start | bytes 24580
  1.3 33.2 %copy-start.4 = (f32[8,128]{1,0:T(8,128)S(1)}, f32[8,128]{1,0:T(8,128)}, u32[]{:S(2)}) copy-start(f32[8,128]{1,0:T(8,128)} %vf_ref.1) | copy-start | bytes 12292
  1.3 33.2 %copy-start.5 = (f32[8,128]{1,0:T(8,128)S(1)}, f32[8,128]{1,0:T(8,128)}, u32[]{:S(2)}) copy-start(f32[8,128]{1,0:T(8,128)} %vs_ref.1) | copy-start | bytes 12292
